TPU v7x, 32 devices: a whole 2x2x4 slice. The times are simulated.
32 devices in a mesh: rep: 2 (over x), fs: 8 (over z, y), tp: 2 (over core).
Axes of the slice: x: 2, y: 2, z: 4, core: 2. Of those that a mesh axis runs over, the one named last changes fastest.
Arguments:
- inputs: bfloat16 [6144, 2048], P(('rep', 'fs')), may hold values from -6 to 6
- w_up: bfloat16 [2048, 4096], P('fs', 'tp'), may hold values from -0.125 to 0.125
- w_down: bfloat16 [4096, 2048], P('tp', 'fs'), may hold values from -0.09375 to 0.09375
- cotangent: bfloat16 [6144, 2048], P(('rep', 'fs')), may hold values from -6 to 6
Outputs:
- d_inputs: bfloat16 [6144, 2048], P(('rep', 'fs'))
- d_w_up: float32 [2048, 4096], P('fs', 'tp')
All inputs are finite; a program needn't handle non-finite values.
Results may differ from a plain program's by a relative error of at most 0.014.
Values may be sent and summed in bfloat16 or wider, within the bound.
A program may use at most 128 MiB of HBM per device.

v0:
```python
import jax
import jax.numpy as jnp
from jax import lax
from jax.sharding import PartitionSpec as P


def per_device(inputs, w_up, w_down, cotangent):
    n_rep = lax.axis_size("rep")
    rep = lax.axis_index("rep")
    tokens = inputs.shape[0]
    hidden = w_up.shape[1] // n_rep

    def from_rep(value, step):
        return lax.ppermute(value, "rep", [((r + step) % n_rep, r) for r in range(n_rep)])

    up_block = lax.dynamic_slice_in_dim(w_up, rep * hidden, hidden, axis=1)
    down_block = lax.dynamic_slice_in_dim(w_down, rep * hidden, hidden, axis=0)
    up_whole = lax.all_gather(up_block, "fs", axis=0, tiled=True)
    down_whole = lax.all_gather(down_block, "fs", axis=1, tiled=True)
    rows = jnp.concatenate([inputs] + [from_rep(inputs, k) for k in range(1, n_rep)], axis=0)
    cots = jnp.concatenate([cotangent] + [from_rep(cotangent, k) for k in range(1, n_rep)], axis=0)
    preact = jnp.dot(rows, up_whole, preferred_element_type=jnp.float32)
    grad_hidden = lax.dot_general(
        cots, down_whole, (((1,), (1,)), ((), ())), preferred_element_type=jnp.float32
    )
    grad_pre = (2.0 * jnp.maximum(preact, 0.0) * grad_hidden).astype(jnp.bfloat16)
    d_w = lax.dot_general(
        rows, grad_pre, (((0,), (0,)), ((), ())), preferred_element_type=jnp.float32
    ).astype(jnp.bfloat16)
    own_rows = lax.psum_scatter(d_w, "fs", scatter_dimension=0, tiled=True)
    partial_value = lax.dot_general(
        grad_pre, up_whole, (((1,), (1,)), ((), ())), preferred_element_type=jnp.float32
    )
    own = partial_value[:tokens]
    for k in range(1, n_rep):
        mine = partial_value[k * tokens : (k + 1) * tokens].astype(jnp.bfloat16)
        own = own + from_rep(mine, n_rep - k).astype(jnp.float32)
    d_inputs = lax.psum(own.astype(jnp.bfloat16), "tp")
    whole_rows = jnp.zeros((own_rows.shape[0], w_up.shape[1]), jnp.float32)
    for k in range(n_rep):
        block = own_rows if k == 0 else from_rep(own_rows, k)
        at = lax.rem(rep + k, n_rep) * hidden
        whole_rows = lax.dynamic_update_slice_in_dim(
            whole_rows, block.astype(jnp.float32), at, axis=1
        )
    return (d_inputs, whole_rows)


def solution(mesh):
    in_specs = (P(("rep", "fs"), None), P("fs", "tp"), P("tp", "fs"), P(("rep", "fs"), None))
    out_specs = (P(("rep", "fs"), None), P("fs", "tp"))
    return jax.shard_map(
        per_device, mesh=mesh, in_specs=in_specs, out_specs=out_specs, check_vma=False
    )
```

profile of v0, /device:TPU:0, one launch (start us, length us, event | category | flops | bytes accessed | tf_op | source)
XLA Modules:
  0.0 296.0 jit_solution(13149260380039072654)
XLA Ops:
  7.2 0.0 copy-start
  7.2 0.0 copy-start.2
  7.2 0.0 all-gather.3.cloned.1.call-start
  7.2 1.2 copy-done
  8.4 0.8 constant_dynamic-slice_fusion.1
  9.2 0.0 all-gather.3.cloned.1.call-update
  9.3 0.0 all-gather.5.cloned.1.call-start
  9.3 1.9 constant_dynamic-slice_fusion
  11.2 0.0 all-gather.5.cloned.1.call-update
  11.2 0.0 reduce-scatter.2.cloned.1.call-start
  11.3 0.0 copy-done.2
  11.3 3.0 %collective-permute-start = (bf16[384,2048]{1,0:T(8,128)(2,1)S(1)}, bf16[384,2048]{1,0:T(8,128)(2,1)S(1)}, u32[]{:S(2)}, u32[]{:S(2)}) collective-permute-start(bf16[384,2048]{1,0:T(8,128)(2,1)S(1)} %copy-done.2), channel_id=1, source_target_pairs={{16,0},{0,16},{17,1},{1,17},{18,2},{2,18},{19,3},{3,19},{20,4},{4,... | collective-permute-start | bytes 4718600 | tf_op jit(solution)/shard_map/ppermute | solution.py:14
  14.3 0.1 collective-permute-start.1
  14.4 1.3 constant_dynamic-update-slice_fusion.1
  15.7 33.8 %collective-permute-done = bf16[384,2048]{1,0:T(8,128)(2,1)S(1)} collective-permute-done((bf16[384,2048]{1,0:T(8,128)(2,1)S(1)}, bf16[384,2048]{1,0:T(8,128)(2,1)S(1)}, u32[]{:S(2)}, u32[]{:S(2)}) %collective-permute-start) | collective-permute-done | bytes 1572896 | tf_op jit(solution)/shard_map/ppermute | solution.py:14
  49.5 1.3 constant_dynamic-update-slice_fusion
  50.8 0.0 copy-start.3
  50.8 35.4 %all-gather.3.cloned.1.call-done = bf16[2048,1024]{1,0:T(8,128)(2,1)} async-done(((bf16[256,1024]{1,0:T(8,128)(2,1)}), bf16[2048,1024]{1,0:T(8,128)(2,1)}) %all-gather.3.cloned.1.call-update) | async-done | bytes 4194320 | tf_op jit(solution)/shard_map/all_gather | solution.py:18
  86.2 8.3 %fusion.8 = f32[768,1024]{1,0:T(8,128)} fusion(bf16[768,2048]{1,0:T(8,128)(2,1)} %constant_dynamic-update-slice_fusion, bf16[2048,1024]{1,0:T(8,128)(2,1)} %all-gather.3.cloned.1.call-done), kind=kOutput, calls=%fused_computation.16 | convolution fusion | flops 3221225472 | bytes 10485760 | tf_op jit(solution)/shard_map/dot_general | solution.py:22
  94.5 0.0 collective-permute-done.1
  94.5 67.5 %all-gather.5.cloned.1.call-done = bf16[1024,2048]{1,0:T(8,128)(2,1)} async-done(((bf16[1024,256]{1,0:T(8,128)(2,1)}), bf16[1024,2048]{1,0:T(8,128)(2,1)}) %all-gather.5.cloned.1.call-update) | async-done | bytes 4194320 | tf_op jit(solution)/shard_map/all_gather | solution.py:19
  162.1 0.0 copy-done.3
  162.1 7.1 %multiply_convert_fusion = bf16[768,1024]{1,0:T(8,128)(2,1)S(1)} fusion(f32[768,1024]{1,0:T(8,128)} %fusion.8, bf16[1024,2048]{1,0:T(8,128)(2,1)} %all-gather.5.cloned.1.call-done, bf16[384,2048]{1,0:T(8,128)(2,1)} %collective-permute-done.1, bf16[384,2048]{1,0:T(8,128)(2,1)S(1)} %copy-done.3), kind=kOutput, calls=%fused_computation.8 | convolution fusion | flops 3230662656 | bytes 12058624 | tf_op jit(solution)/shard_map/dot_general | solution.py:23
  169.1 0.0 copy-start.4
  169.2 1.1 copy-done.4
  170.3 7.0 %convolution_convert_fusion = bf16[2048,1024]{1,0:T(8,128)(2,1)} fusion(bf16[768,2048]{1,0:T(8,128)(2,1)} %constant_dynamic-update-slice_fusion, bf16[768,1024]{1,0:T(8,128)(2,1)S(1)} %multiply_convert_fusion), kind=kOutput, calls=%fused_computation | convolution fusion | flops 3223322624 | bytes 8912896 | tf_op jit(solution)/shard_map/dot_general | solution.py:27
  177.3 0.0 copy-start.5
  177.3 0.0 reduce-scatter.2.cloned.1.call-update
  177.4 0.0 all-reduce.2.cloned.1.call-start
  177.4 1.3 copy-done.5
  178.7 5.3 %fusion.9 = f32[768,2048]{1,0:T(8,128)S(1)} fusion(bf16[768,1024]{1,0:T(8,128)(2,1)S(1)} %copy-done.5, bf16[2048,1024]{1,0:T(8,128)(2,1)} %all-gather.3.cloned.1.call-done), kind=kOutput, calls=%fused_computation.17 | convolution fusion | flops 3221225472 | bytes 12058624 | tf_op jit(solution)/shard_map/dot_general | solution.py:31
  184.0 0.2 slice.15
  184.2 1.6 collective-permute-start.2
  185.8 33.9 %collective-permute-done.2 = bf16[384,2048]{1,0:T(8,128)(2,1)S(1)} collective-permute-done((bf16[384,2048]{1,0:T(8,128)(2,1)S(1)}, bf16[384,2048]{1,0:T(8,128)(2,1)S(1)}, u32[]{:S(2)}, u32[]{:S(2)}) %collective-permute-start.2) | collective-permute-done | bytes 1572896 | tf_op jit(solution)/shard_map/ppermute | solution.py:14
  219.7 1.7 fusion
  221.4 0.0 all-reduce.2.cloned.1.call-update
  221.4 42.5 %reduce-scatter.2.cloned.1.call-done = bf16[256,1024]{1,0:T(8,128)(2,1)} async-done(((bf16[2048,1024]{1,0:T(8,128)(2,1)}), bf16[256,1024]{1,0:T(8,128)(2,1)}) %reduce-scatter.2.cloned.1.call-update) | async-done | bytes 524304 | tf_op jit(solution)/shard_map/reduce_scatter | solution.py:30
  263.9 1.5 collective-permute-start.3
  265.4 0.2 broadcast_in_dim.3
  265.6 1.2 convert_dynamic-update-slice_fusion.1
  266.8 10.8 %collective-permute-done.3 = bf16[256,1024]{1,0:T(8,128)(2,1)} collective-permute-done((bf16[256,1024]{1,0:T(8,128)(2,1)}, bf16[256,1024]{1,0:T(8,128)(2,1)}, u32[]{:S(2)}, u32[]{:S(2)}) %collective-permute-start.3) | collective-permute-done | bytes 524320 | tf_op jit(solution)/shard_map/ppermute | solution.py:14
  277.6 1.1 convert_dynamic-update-slice_fusion
  278.7 0.0 copy-start.1
  278.7 8.0 %all-reduce.2.cloned.1.call-done = bf16[384,2048]{1,0:T(8,128)(2,1)} async-done(((bf16[384,2048]{1,0:T(8,128)(2,1)}), bf16[384,2048]{1,0:T(8,128)(2,1)}) %all-reduce.2.cloned.1.call-update) | async-done | bytes 1572880 | tf_op jit(solution)/shard_map/psum | solution.py:38
  286.7 2.7 copy.10
  289.5 0.0 copy-done.1
Async XLA Ops:
  7.2 1.2 copy-start
  7.2 4.1 %copy-start.2 = (bf16[384,2048]{1,0:T(8,128)(2,1)S(1)}, bf16[384,2048]{1,0:T(8,128)(2,1)}, u32[]{:S(2)}) copy-start(bf16[384,2048]{1,0:T(8,128)(2,1)} %param.4) | copy-start | bytes 4718596
  7.2 79.1 %all-gather.3.cloned.1.call-start = ((), (), s32[]{:S(2)}) async-start(), calls=%async_computation.1 | async-start | bytes 4718592 | tf_op jit(solution)/shard_map/all_gather | solution.py:18
  9.3 152.8 %all-gather.5.cloned.1.call-start = ((), (), s32[]{:S(2)}) async-start(), calls=%async_computation.2 | async-start | bytes 4718592 | tf_op jit(solution)/shard_map/all_gather | solution.py:19
  11.2 252.7 %reduce-scatter.2.cloned.1.call-start = ((), (), s32[]{:S(2)}) async-start(), calls=%async_computation.4 | async-start | bytes 4718592 | tf_op jit(solution)/shard_map/reduce_scatter | solution.py:30
  11.3 38.3 %collective-permute-start = (bf16[384,2048]{1,0:T(8,128)(2,1)S(1)}, bf16[384,2048]{1,0:T(8,128)(2,1)S(1)}, u32[]{:S(2)}, u32[]{:S(2)}) collective-permute-start(bf16[384,2048]{1,0:T(8,128)(2,1)S(1)} %copy-done.2), channel_id=1, source_target_pairs={{16,0},{0,16},{17,1},{1,17},{18,2},{2,18},{19,3},{3,19},{20,4},{4,... | collective-permute-start | bytes 4718600 | tf_op jit(solution)/shard_map/ppermute | solution.py:14
  14.3 80.2 %collective-permute-start.1 = (bf16[384,2048]{1,0:T(8,128)(2,1)}, bf16[384,2048]{1,0:T(8,128)(2,1)}, u32[]{:S(2)}, u32[]{:S(2)}) collective-permute-start(bf16[384,2048]{1,0:T(8,128)(2,1)} %param.7), channel_id=1, source_target_pairs={{16,0},{0,16},{17,1},{1,17},{18,2},{2,18},{19,3},{3,19},{20,4},{4,... | collective-permute-start | bytes 4718600 | tf_op jit(solution)/shard_map/ppermute | solution.py:14
  50.8 111.3 %copy-start.3 = (bf16[384,2048]{1,0:T(8,128)(2,1)S(1)}, bf16[384,2048]{1,0:T(8,128)(2,1)}, u32[]{:S(2)}) copy-start(bf16[384,2048]{1,0:T(8,128)(2,1)} %param.7) | copy-start | bytes 4718596
  169.1 1.1 copy-start.4
  177.3 1.4 copy-start.5
  177.4 109.4 %all-reduce.2.cloned.1.call-start = ((), (), s32[]{:S(2)}) async-start(), calls=%async_computation.3 | async-start | bytes 3145728 | tf_op jit(solution)/shard_map/psum | solution.py:38
  184.2 35.5 %collective-permute-start.2 = (bf16[384,2048]{1,0:T(8,128)(2,1)S(1)}, bf16[384,2048]{1,0:T(8,128)(2,1)S(1)}, u32[]{:S(2)}, u32[]{:S(2)}) collective-permute-start(bf16[384,2048]{1,0:T(8,128)(2,1)S(1)} %slice.15), channel_id=1, source_target_pairs={{16,0},{0,16},{17,1},{1,17},{18,2},{2,18},{19,3},{3,19},{20,4},{4,... | collective-permute-start | bytes 4718600 | tf_op jit(solution)/shard_map/ppermute | solution.py:14
  263.9 13.6 %collective-permute-start.3 = (bf16[256,1024]{1,0:T(8,128)(2,1)}, bf16[256,1024]{1,0:T(8,128)(2,1)}, u32[]{:S(2)}, u32[]{:S(2)}) collective-permute-start(bf16[256,1024]{1,0:T(8,128)(2,1)} %reduce-scatter.2.cloned.1.call-done), channel_id=1, source_target_pairs={{16,0},{0,16},{17,1},{1,17},{18,2},{2,18},{19,3},{3,19},{20,4},{4,... | collective-permute-start | bytes 1572872 | tf_op jit(solution)/shard_map/ppermute | solution.py:14
  278.7 10.8 %copy-start.1 = (f32[256,2048]{1,0:T(8,128)}, f32[256,2048]{1,0:T(8,128)S(1)}, u32[]{:S(2)}) copy-start(f32[256,2048]{1,0:T(8,128)S(1)} %convert_dynamic-update-slice_fusion) | copy-start | bytes 6291460
Sparse Core Ops, SparseCore 0:
  10.7 75.5 all-gather.2
  88.9 73.1 all-gather.4
  177.5 86.4 reduce-scatter.1
  266.7 19.9 all-reduce.1
where the time goes:
time: 296 us
  waiting for transfers between devices  232 us (78%)
  matrix products  27.7 us (9%)
  between operations  13.9 us (5%)
  local copies, waits for them, and re-layouts  12.1 us (4%)
  starting transfers between devices  6.32 us (2%)
  other arithmetic  4.01 us (1%)
    ppermute x4, waiting for transfers between devices, from_rep(): lax.ppermute(value, 'rep', [((r + step) % n_rep, r) for r in range(n_rep)])  78.5 us
    all_gather x1, waiting for transfers between devices, per_device(): down_whole = lax.all_gather(down_block, 'fs', axis=1, tiled=True)  67.5 us
    reduce_scatter x1, waiting for transfers between devices, per_device(): own_rows = lax.psum_scatter(d_w, 'fs', scatter_dimension=0, tiled=True)  42.5 us
    all_gather x1, waiting for transfers between devices, per_device(): up_whole = lax.all_gather(up_block, 'fs', axis=0, tiled=True)  35.4 us
    dot_general x1, matrix products, per_device(): preact = jnp.dot(rows, up_whole, preferred_element_type=jnp.float32)  8.28 us
    psum x1, waiting for transfers between devices, per_device(): d_inputs = lax.psum(own.astype(jnp.bfloat16), 'tp')  8.01 us
    unnamed x14, local copies, waits for them, and re-layouts  7.72 us
    dot_general x1, matrix products, per_device(): lax.dot_general(cots, down_whole, (((1,), (1,)), ((), ())), preferred_ele...  7.07 us
  transfers between devices with their start and end apart: 8, of which 7 were waited for; matrix products, arithmetic and copies ran while one was open for 8% of the time, Pallas kernels for 0%

commit v1 on v0

--- a/solution.py
+++ b/solution.py
@@ -15,7 +15,21 @@
 
     up_block = lax.dynamic_slice_in_dim(w_up, rep * hidden, hidden, axis=1)
     down_block = lax.dynamic_slice_in_dim(w_down, rep * hidden, hidden, axis=0)
-    up_whole = lax.all_gather(up_block, "fs", axis=0, tiled=True)
+    ways, here, step_2 = (lax.axis_size("fs"), lax.axis_index("fs"), up_block.shape[0])
+    lengths = [n * ways if d == 0 else n for d, n in enumerate(up_block.shape)]
+    full = lax.dynamic_update_slice_in_dim(
+        jnp.zeros(lengths, up_block.dtype), up_block, here * step_2, axis=0
+    )
+    going_up = going_down = up_block
+    for far in range(1, ways // 2 + 1):
+        going_up = lax.ppermute(going_up, "fs", [(d, (d + 1) % ways) for d in range(ways)])
+        full = lax.dynamic_update_slice_in_dim(full, going_up, (here - far) % ways * step_2, axis=0)
+        if 2 * far < ways:
+            going_down = lax.ppermute(going_down, "fs", [(d, (d - 1) % ways) for d in range(ways)])
+            full = lax.dynamic_update_slice_in_dim(
+                full, going_down, (here + far) % ways * step_2, axis=0
+            )
+    up_whole = full
     down_whole = lax.all_gather(down_block, "fs", axis=1, tiled=True)
     rows = jnp.concatenate([inputs] + [from_rep(inputs, k) for k in range(1, n_rep)], axis=0)
     cots = jnp.concatenate([cotangent] + [from_rep(cotangent, k) for k in range(1, n_rep)], axis=0)

time: 296 us -> 275 us (0.929)
  waiting for transfers between devices: 232 us -> 183 us
  starting transfers between devices: 6.32 us -> 27.5 us
  local copies, waits for them, and re-layouts: 12.1 us -> 20.9 us
    ppermute x0 -> x7, waiting for transfers between devices: none -> 79.9 us  [the longest x4 79.9 us: per_device(): lax.ppermute(going_up, 'fs', [(d, (d + 1) % ways) for d in range(ways)])]
    all_gather x1, waiting for transfers between devices: 67.5 us -> 7.15 us  [per_device(): down_whole = lax.all_gather(down_block, 'fs', axis=1, tiled=True)]
    all_gather x1 -> x0, waiting for transfers between devices: 35.4 us -> none  [per_device(): up_whole = lax.all_gather(up_block, 'fs', axis=0, tiled=True)]
    ppermute x4, waiting for transfers between devices: 78.5 us -> 45 us  [from_rep(): lax.ppermute(value, 'rep', [((r + step) % n_rep, r) for r in range(n_rep)])]
    ppermute x0 -> x7, starting transfers between devices: none -> 21.2 us  [the longest x3 13.3 us: per_device(): lax.ppermute(going_down, 'fs', [(d, (d - 1) % ways) for d in range(ways)])]
    dynamic_update_slice x0 -> x8, local copies, waits for them, and re-layouts: none -> 9.91 us  [the longest x3 4.58 us: per_device(): lax.dynamic_update_slice_in_dim(full, going_down, (here + far) % ways * s...]
    unnamed x14 -> x18, local copies, waits for them, and re-layouts: 7.72 us -> 5.65 us
  transfers between devices with their start and end apart: 8 -> 14, of which waited for: 7 -> 9; matrix products, arithmetic and copies ran while one was open for 8% -> 12% of each run, Pallas kernels for 0% -> 0%
where the time goes in v1:
time: 275 us
  waiting for transfers between devices  183 us (67%)
  starting transfers between devices  27.5 us (10%)
  matrix products  25.7 us (9%)
  local copies, waits for them, and re-layouts  20.9 us (8%)
  between operations  13.9 us (5%)
  other arithmetic  3.94 us (1%)
    ppermute x4, waiting for transfers between devices, per_device(): lax.ppermute(going_up, 'fs', [(d, (d + 1) % ways) for d in range(ways)])  79.9 us
    ppermute x4, waiting for transfers between devices, from_rep(): lax.ppermute(value, 'rep', [((r + step) % n_rep, r) for r in range(n_rep)])  45 us
    reduce_scatter x1, waiting for transfers between devices, per_device(): own_rows = lax.psum_scatter(d_w, 'fs', scatter_dimension=0, tiled=True)  42.3 us
    ppermute x3, starting transfers between devices, per_device(): lax.ppermute(going_down, 'fs', [(d, (d - 1) % ways) for d in range(ways)])  13.3 us
    psum x1, waiting for transfers between devices, per_device(): d_inputs = lax.psum(own.astype(jnp.bfloat16), 'tp')  8.19 us
    ppermute x4, starting transfers between devices, per_device(): lax.ppermute(going_up, 'fs', [(d, (d + 1) % ways) for d in range(ways)])  7.92 us
    dot_general x1, matrix products, per_device(): preact = jnp.dot(rows, up_whole, preferred_element_type=jnp.float32)  7.32 us
    all_gather x1, waiting for transfers between devices, per_device(): down_whole = lax.all_gather(down_block, 'fs', axis=1, tiled=True)  7.15 us
  transfers between devices with their start and end apart: 14, of which 9 were waited for; matrix products, arithmetic and copies ran while one was open for 12% of the time, Pallas kernels for 0%

profile of v1, /device:TPU:0, one launch (start us, length us, event | category | flops | bytes accessed | tf_op | source)
XLA Modules:
  0.0 274.5 jit_solution(11084528928403061623)
XLA Ops:
  7.2 0.0 copy-start
  7.2 0.0 all-gather.2.cloned.1.call-start
  7.2 1.2 copy-done
  8.4 0.8 constant_dynamic-slice_fusion
  9.2 0.0 all-gather.2.cloned.1.call-update
  9.2 0.0 reduce-scatter.2.cloned.1.call-start
  9.3 0.0 copy-start.5
  9.3 2.5 broadcast_in_dim.6
  11.9 0.0 copy-done.5
  11.9 0.9 constant_dynamic-update-slice_fusion.9
  12.8 3.0 %collective-permute-start.1 = (bf16[256,1024]{1,0:T(8,128)(2,1)S(1)}, bf16[256,1024]{1,0:T(8,128)(2,1)S(1)}, u32[]{:S(2)}, u32[]{:S(2)}) collective-permute-start(bf16[256,1024]{1,0:T(8,128)(2,1)S(1)} %get-tuple-element.3), channel_id=1, source_target_pairs={{0,2},{2,4},{4,6},{6,8},{8,10},{10,12},{12,14},{14,0},{1,3},{3,5},... | collective-permute-start | bytes 1572872 | tf_op jit(solution)/shard_map/ppermute | solution.py:25
  15.8 3.1 %collective-permute-start.2 = (bf16[256,1024]{1,0:T(8,128)(2,1)S(1)}, bf16[256,1024]{1,0:T(8,128)(2,1)}, u32[]{:S(2)}, u32[]{:S(2)}) collective-permute-start(bf16[256,1024]{1,0:T(8,128)(2,1)S(1)} %get-tuple-element.3), channel_id=1, source_target_pairs={{0,14},{2,0},{4,2},{6,4},{8,6},{10,8},{12,10},{14,12},{1,15},{3,1}... | collective-permute-start | bytes 1572872 | tf_op jit(solution)/shard_map/ppermute | solution.py:28
  18.9 0.0 copy-done.2
  18.9 1.6 collective-permute-start
  20.5 23.3 %collective-permute-done.1 = bf16[256,1024]{1,0:T(8,128)(2,1)S(1)} collective-permute-done((bf16[256,1024]{1,0:T(8,128)(2,1)S(1)}, bf16[256,1024]{1,0:T(8,128)(2,1)S(1)}, u32[]{:S(2)}, u32[]{:S(2)}) %collective-permute-start.1) | collective-permute-done | bytes 524320 | tf_op jit(solution)/shard_map/ppermute | solution.py:25
  43.8 2.5 collective-permute-start.3
  46.3 0.0 collective-permute-done.2
  46.3 3.1 %collective-permute-start.4 = (bf16[256,1024]{1,0:T(8,128)(2,1)}, bf16[256,1024]{1,0:T(8,128)(2,1)}, u32[]{:S(2)}, u32[]{:S(2)}) collective-permute-start(bf16[256,1024]{1,0:T(8,128)(2,1)} %collective-permute-done.2), channel_id=1, source_target_pairs={{0,14},{2,0},{4,2},{6,4},{8,6},{10,8},{12,10},{14,12},{1,15},{3,1}... | collective-permute-start | bytes 1572872 | tf_op jit(solution)/shard_map/ppermute | solution.py:28
  49.4 1.5 collective-permute-start.8
  50.9 19.6 %collective-permute-done.3 = bf16[256,1024]{1,0:T(8,128)(2,1)} collective-permute-done((bf16[256,1024]{1,0:T(8,128)(2,1)S(1)}, bf16[256,1024]{1,0:T(8,128)(2,1)}, u32[]{:S(2)}, u32[]{:S(2)}) %collective-permute-start.3) | collective-permute-done | bytes 524320 | tf_op jit(solution)/shard_map/ppermute | solution.py:25
  70.4 0.1 collective-permute-start.5
  70.5 0.1 constant_dynamic-update-slice_fusion.1
  70.6 0.0 collective-permute-done.4
  70.7 7.1 %collective-permute-start.6 = (bf16[256,1024]{1,0:T(8,128)(2,1)}, bf16[256,1024]{1,0:T(8,128)(2,1)S(1)}, u32[]{:S(2)}, u32[]{:S(2)}) collective-permute-start(bf16[256,1024]{1,0:T(8,128)(2,1)} %collective-permute-done.4), channel_id=1, source_target_pairs={{0,14},{2,0},{4,2},{6,4},{8,6},{10,8},{12,10},{14,12},{1,15},{3,1}... | collective-permute-start | bytes 1572872 | tf_op jit(solution)/shard_map/ppermute | solution.py:28
  77.7 0.9 constant_dynamic-update-slice_fusion.8
  78.6 1.9 constant_dynamic-update-slice_fusion.7
  80.5 1.9 constant_dynamic-update-slice_fusion.6
  82.3 22.1 %collective-permute-done.5 = bf16[256,1024]{1,0:T(8,128)(2,1)S(1)} collective-permute-done((bf16[256,1024]{1,0:T(8,128)(2,1)}, bf16[256,1024]{1,0:T(8,128)(2,1)S(1)}, u32[]{:S(2)}, u32[]{:S(2)}) %collective-permute-start.5) | collective-permute-done | bytes 524320 | tf_op jit(solution)/shard_map/ppermute | solution.py:25
  104.4 2.4 collective-permute-start.7
  106.8 1.9 constant_dynamic-update-slice_fusion.5
  108.7 0.8 constant_dynamic-update-slice_fusion.4
  109.5 0.0 collective-permute-done.6
  109.5 0.9 constant_dynamic-update-slice_fusion.3
  110.3 0.0 collective-permute-done
  110.3 1.5 constant_dynamic-update-slice_fusion
  111.9 0.0 copy-start.3
  111.9 14.9 %collective-permute-done.7 = bf16[256,1024]{1,0:T(8,128)(2,1)S(1)} collective-permute-done((bf16[256,1024]{1,0:T(8,128)(2,1)S(1)}, bf16[256,1024]{1,0:T(8,128)(2,1)S(1)}, u32[]{:S(2)}, u32[]{:S(2)}) %collective-permute-start.7) | collective-permute-done | bytes 524320 | tf_op jit(solution)/shard_map/ppermute | solution.py:25
  126.8 0.8 constant_dynamic-update-slice_fusion.2
  127.6 7.3 %fusion.15 = f32[768,1024]{1,0:T(8,128)} fusion(bf16[768,2048]{1,0:T(8,128)(2,1)S(1)} %constant_dynamic-update-slice_fusion, bf16[2048,1024]{1,0:T(8,128)(2,1)} %constant_dynamic-update-slice_fusion.2), kind=kOutput, calls=%fused_computation.33 | convolution fusion | flops 3221225472 | bytes 10485760 | tf_op jit(solution)/shard_map/dot_general | solution.py:36
  134.9 0.0 copy-done.3
  134.9 0.0 collective-permute-done.8
  134.9 7.2 %all-gather.2.cloned.1.call-done = bf16[1024,2048]{1,0:T(8,128)(2,1)} async-done(((bf16[1024,256]{1,0:T(8,128)(2,1)}), bf16[1024,2048]{1,0:T(8,128)(2,1)}) %all-gather.2.cloned.1.call-update) | async-done | bytes 4194320 | tf_op jit(solution)/shard_map/all_gather | solution.py:33
  142.1 6.3 %fusion.1 = f32[768,1024]{1,0:T(8,128)S(1)} fusion(bf16[1024,2048]{1,0:T(8,128)(2,1)} %all-gather.2.cloned.1.call-done, bf16[384,2048]{1,0:T(8,128)(2,1)} %collective-permute-done.8, bf16[384,2048]{1,0:T(8,128)(2,1)} %param.7), kind=kOutput, calls=%fused_computation.4 | convolution fusion | flops 3227516928 | bytes 10485760 | tf_op jit(solution)/shard_map/dot_general | solution.py:37
  148.5 0.0 copy-start.7
  148.5 1.6 copy-done.7
  150.1 0.0 copy-done.6
  150.1 5.2 %convolution_convert_fusion = bf16[2048,1024]{1,0:T(8,128)(2,1)} fusion(bf16[768,2048]{1,0:T(8,128)(2,1)S(1)} %copy-done.4, f32[768,1024]{1,0:T(8,128)S(1)} %fusion.1, f32[768,1024]{1,0:T(8,128)S(1)} %copy-done.6), kind=kOutput, calls=%fused_computation | convolution fusion | flops 3226468352 | bytes 13631488 | tf_op jit(solution)/shard_map/dot_general | solution.py:41
  155.3 0.0 reduce-scatter.2.cloned.1.call-update
  155.3 0.0 all-reduce.2.cloned.1.call-start
  155.4 6.9 %fusion.5 = f32[768,2048]{1,0:T(8,128)S(1)} fusion(bf16[2048,1024]{1,0:T(8,128)(2,1)} %constant_dynamic-update-slice_fusion.2, f32[768,1024]{1,0:T(8,128)} %copy-done.7, f32[768,1024]{1,0:T(8,128)} %fusion.15), kind=kOutput, calls=%fused_computation.9 | convolution fusion | flops 3224371200 | bytes 16777216 | tf_op jit(solution)/shard_map/dot_general | solution.py:45
  162.3 0.2 slice.15
  162.5 1.6 collective-permute-start.9
  164.0 34.3 %collective-permute-done.9 = bf16[384,2048]{1,0:T(8,128)(2,1)S(1)} collective-permute-done((bf16[384,2048]{1,0:T(8,128)(2,1)S(1)}, bf16[384,2048]{1,0:T(8,128)(2,1)S(1)}, u32[]{:S(2)}, u32[]{:S(2)}) %collective-permute-start.9) | collective-permute-done | bytes 1572896 | tf_op jit(solution)/shard_map/ppermute | solution.py:14
  198.3 1.6 fusion
  200.0 0.0 all-reduce.2.cloned.1.call-update
  200.0 42.3 %reduce-scatter.2.cloned.1.call-done = bf16[256,1024]{1,0:T(8,128)(2,1)} async-done(((bf16[2048,1024]{1,0:T(8,128)(2,1)}), bf16[256,1024]{1,0:T(8,128)(2,1)}) %reduce-scatter.2.cloned.1.call-update) | async-done | bytes 524304 | tf_op jit(solution)/shard_map/reduce_scatter | solution.py:44
  242.3 1.5 collective-permute-start.10
  243.8 0.2 broadcast_in_dim.7
  244.0 1.2 convert_dynamic-update-slice_fusion.1
  245.2 10.7 %collective-permute-done.10 = bf16[256,1024]{1,0:T(8,128)(2,1)} collective-permute-done((bf16[256,1024]{1,0:T(8,128)(2,1)}, bf16[256,1024]{1,0:T(8,128)(2,1)}, u32[]{:S(2)}, u32[]{:S(2)}) %collective-permute-start.10) | collective-permute-done | bytes 524320 | tf_op jit(solution)/shard_map/ppermute | solution.py:14
  255.9 1.1 convert_dynamic-update-slice_fusion
  257.1 0.0 copy-start.1
  257.1 8.2 %all-reduce.2.cloned.1.call-done = bf16[384,2048]{1,0:T(8,128)(2,1)} async-done(((bf16[384,2048]{1,0:T(8,128)(2,1)}), bf16[384,2048]{1,0:T(8,128)(2,1)}) %all-reduce.2.cloned.1.call-update) | async-done | bytes 1572880 | tf_op jit(solution)/shard_map/psum | solution.py:52
  265.3 2.7 copy.18
  (5 shorter events, 0.0 us)
Async XLA Ops:
  7.2 1.2 copy-start
  7.2 134.9 %all-gather.2.cloned.1.call-start = ((), (), s32[]{:S(2)}) async-start(), calls=%async_computation.1 | async-start | bytes 4718592 | tf_op jit(solution)/shard_map/all_gather | solution.py:33
  9.2 9.6 %copy-start.2 = (bf16[384,2048]{1,0:T(8,128)(2,1)S(1)}, bf16[384,2048]{1,0:T(8,128)(2,1)}, u32[]{:S(2)}) copy-start(bf16[384,2048]{1,0:T(8,128)(2,1)} %param.4) | copy-start | bytes 4718596
  9.2 233.1 %reduce-scatter.2.cloned.1.call-start = ((), (), s32[]{:S(2)}) async-start(), calls=%async_computation.3 | async-start | bytes 4718592 | tf_op jit(solution)/shard_map/reduce_scatter | solution.py:44
  9.3 2.6 copy-start.5
  12.8 31.0 %collective-permute-start.1 = (bf16[256,1024]{1,0:T(8,128)(2,1)S(1)}, bf16[256,1024]{1,0:T(8,128)(2,1)S(1)}, u32[]{:S(2)}, u32[]{:S(2)}) collective-permute-start(bf16[256,1024]{1,0:T(8,128)(2,1)S(1)} %get-tuple-element.3), channel_id=1, source_target_pairs={{0,2},{2,4},{4,6},{6,8},{8,10},{10,12},{12,14},{14,0},{1,3},{3,5},... | collective-permute-start | bytes 1572872 | tf_op jit(solution)/shard_map/ppermute | solution.py:25
  15.8 30.5 %collective-permute-start.2 = (bf16[256,1024]{1,0:T(8,128)(2,1)S(1)}, bf16[256,1024]{1,0:T(8,128)(2,1)}, u32[]{:S(2)}, u32[]{:S(2)}) collective-permute-start(bf16[256,1024]{1,0:T(8,128)(2,1)S(1)} %get-tuple-element.3), channel_id=1, source_target_pairs={{0,14},{2,0},{4,2},{6,4},{8,6},{10,8},{12,10},{14,12},{1,15},{3,1}... | collective-permute-start | bytes 1572872 | tf_op jit(solution)/shard_map/ppermute | solution.py:28
  18.9 91.5 %collective-permute-start = (bf16[384,2048]{1,0:T(8,128)(2,1)S(1)}, bf16[384,2048]{1,0:T(8,128)(2,1)}, u32[]{:S(2)}, u32[]{:S(2)}) collective-permute-start(bf16[384,2048]{1,0:T(8,128)(2,1)S(1)} %copy-done.2), channel_id=1, source_target_pairs={{16,0},{0,16},{17,1},{1,17},{18,2},{2,18},{19,3},{3,19},{20,4},{4,... | collective-permute-start | bytes 4718600 | tf_op jit(solution)/shard_map/ppermute | solution.py:14
  43.8 26.6 %collective-permute-start.3 = (bf16[256,1024]{1,0:T(8,128)(2,1)S(1)}, bf16[256,1024]{1,0:T(8,128)(2,1)}, u32[]{:S(2)}, u32[]{:S(2)}) collective-permute-start(bf16[256,1024]{1,0:T(8,128)(2,1)S(1)} %collective-permute-done.1), channel_id=1, source_target_pairs={{0,2},{2,4},{4,6},{6,8},{8,10},{10,12},{12,14},{14,0},{1,3},{3,5},... | collective-permute-start | bytes 1572872 | tf_op jit(solution)/shard_map/ppermute | solution.py:25
  46.3 24.4 %collective-permute-start.4 = (bf16[256,1024]{1,0:T(8,128)(2,1)}, bf16[256,1024]{1,0:T(8,128)(2,1)}, u32[]{:S(2)}, u32[]{:S(2)}) collective-permute-start(bf16[256,1024]{1,0:T(8,128)(2,1)} %collective-permute-done.2), channel_id=1, source_target_pairs={{0,14},{2,0},{4,2},{6,4},{8,6},{10,8},{12,10},{14,12},{1,15},{3,1}... | collective-permute-start | bytes 1572872 | tf_op jit(solution)/shard_map/ppermute | solution.py:28
  49.4 85.6 %collective-permute-start.8 = (bf16[384,2048]{1,0:T(8,128)(2,1)}, bf16[384,2048]{1,0:T(8,128)(2,1)}, u32[]{:S(2)}, u32[]{:S(2)}) collective-permute-start(bf16[384,2048]{1,0:T(8,128)(2,1)} %param.7), channel_id=1, source_target_pairs={{16,0},{0,16},{17,1},{1,17},{18,2},{2,18},{19,3},{3,19},{20,4},{4,... | collective-permute-start | bytes 4718600 | tf_op jit(solution)/shard_map/ppermute | solution.py:14
  70.4 34.0 %collective-permute-start.5 = (bf16[256,1024]{1,0:T(8,128)(2,1)}, bf16[256,1024]{1,0:T(8,128)(2,1)S(1)}, u32[]{:S(2)}, u32[]{:S(2)}) collective-permute-start(bf16[256,1024]{1,0:T(8,128)(2,1)} %collective-permute-done.3), channel_id=1, source_target_pairs={{0,2},{2,4},{4,6},{6,8},{8,10},{10,12},{12,14},{14,0},{1,3},{3,5},... | collective-permute-start | bytes 1572872 | tf_op jit(solution)/shard_map/ppermute | solution.py:25
  70.7 38.8 %collective-permute-start.6 = (bf16[256,1024]{1,0:T(8,128)(2,1)}, bf16[256,1024]{1,0:T(8,128)(2,1)S(1)}, u32[]{:S(2)}, u32[]{:S(2)}) collective-permute-start(bf16[256,1024]{1,0:T(8,128)(2,1)} %collective-permute-done.4), channel_id=1, source_target_pairs={{0,14},{2,0},{4,2},{6,4},{8,6},{10,8},{12,10},{14,12},{1,15},{3,1}... | collective-permute-start | bytes 1572872 | tf_op jit(solution)/shard_map/ppermute | solution.py:28
  104.4 22.4 %collective-permute-start.7 = (bf16[256,1024]{1,0:T(8,128)(2,1)S(1)}, bf16[256,1024]{1,0:T(8,128)(2,1)S(1)}, u32[]{:S(2)}, u32[]{:S(2)}) collective-permute-start(bf16[256,1024]{1,0:T(8,128)(2,1)S(1)} %collective-permute-done.5), channel_id=1, source_target_pairs={{0,2},{2,4},{4,6},{6,8},{8,10},{10,12},{12,14},{14,0},{1,3},{3,5},... | collective-permute-start | bytes 1572872 | tf_op jit(solution)/shard_map/ppermute | solution.py:25
  111.9 23.1 %copy-start.3 = (bf16[768,2048]{1,0:T(8,128)(2,1)}, bf16[768,2048]{1,0:T(8,128)(2,1)S(1)}, u32[]{:S(2)}) copy-start(bf16[768,2048]{1,0:T(8,128)(2,1)S(1)} %constant_dynamic-update-slice_fusion) | copy-start | bytes 9437188
  142.1 8.0 %copy-start.4 = (bf16[768,2048]{1,0:T(8,128)(2,1)S(1)}, bf16[768,2048]{1,0:T(8,128)(2,1)}, u32[]{:S(2)}) copy-start(bf16[768,2048]{1,0:T(8,128)(2,1)} %copy-done.3) | copy-start | bytes 9437188
  142.1 8.0 %copy-start.6 = (f32[768,1024]{1,0:T(8,128)S(1)}, f32[768,1024]{1,0:T(8,128)}, u32[]{:S(2)}) copy-start(f32[768,1024]{1,0:T(8,128)} %fusion.15) | copy-start | bytes 9437188
  148.5 1.6 copy-start.7
  155.3 109.9 %all-reduce.2.cloned.1.call-start = ((), (), s32[]{:S(2)}) async-start(), calls=%async_computation.2 | async-start | bytes 3145728 | tf_op jit(solution)/shard_map/psum | solution.py:52
  162.5 35.9 %collective-permute-start.9 = (bf16[384,2048]{1,0:T(8,128)(2,1)S(1)}, bf16[384,2048]{1,0:T(8,128)(2,1)S(1)}, u32[]{:S(2)}, u32[]{:S(2)}) collective-permute-start(bf16[384,2048]{1,0:T(8,128)(2,1)S(1)} %slice.15), channel_id=1, source_target_pairs={{16,0},{0,16},{17,1},{1,17},{18,2},{2,18},{19,3},{3,19},{20,4},{4,... | collective-permute-start | bytes 4718600 | tf_op jit(solution)/shard_map/ppermute | solution.py:14
  242.3 13.6 %collective-permute-start.10 = (bf16[256,1024]{1,0:T(8,128)(2,1)}, bf16[256,1024]{1,0:T(8,128)(2,1)}, u32[]{:S(2)}, u32[]{:S(2)}) collective-permute-start(bf16[256,1024]{1,0:T(8,128)(2,1)} %reduce-scatter.2.cloned.1.call-done), channel_id=1, source_target_pairs={{16,0},{0,16},{17,1},{1,17},{18,2},{2,18},{19,3},{3,19},{20,4},{4,... | collective-permute-start | bytes 1572872 | tf_op jit(solution)/shard_map/ppermute | solution.py:14
  257.1 10.9 %copy-start.1 = (f32[256,2048]{1,0:T(8,128)}, f32[256,2048]{1,0:T(8,128)S(1)}, u32[]{:S(2)}) copy-start(f32[256,2048]{1,0:T(8,128)S(1)} %convert_dynamic-update-slice_fusion) | copy-start | bytes 6291460
Sparse Core Ops, SparseCore 0:
  10.6 131.4 all-gather.1
  155.5 86.8 reduce-scatter.1
  245.2 19.9 all-reduce.1
